TPU v7x, 128 devices: a whole 4x4x4 slice. The times are simulated.
128 devices in a mesh: sp: 16 (over z, y), tp: 8 (over x, core).
Axes of the slice: x: 4, y: 4, z: 4, core: 2. Of those that a mesh axis runs over, the one named last changes fastest.
Arguments:
- residual_in: bfloat16 [12288, 2048], P('sp', 'tp'), may hold values from -11 to 11
- queries: bfloat16 [12288, 1024], P('sp', 'tp'), may hold values from -6 to 6
- keys: bfloat16 [12288, 256], P('sp'), may hold values from -6 to 6
- values: bfloat16 [12288, 256], P('sp'), may hold values from -6 to 6
- query_gain: float32 [128], replicated, may hold values from 1.5 to 5
- key_norm_gain: float32 [128], replicated, may hold values from 1.5 to 5
- out_weight: bfloat16 [1024, 2048], P('tp'), may hold values from -0.1875 to 0.1875
- mlp_gain: float32 [2048], replicated, may hold values from 0.1 to 1.9
- gate_weight: bfloat16 [2048, 5632], P('sp', 'tp'), may hold values from -0.125 to 0.125
- up_weight: bfloat16 [2048, 5632], P('sp', 'tp'), may hold values from -0.125 to 0.125
- down_weight: bfloat16 [5632, 2048], P('tp', 'sp'), may hold values from -0.15625 to 0.15625
Outputs:
- layer_out: bfloat16 [12288, 2048], P('sp', 'tp')
All inputs are finite; a program needn't handle non-finite values.
Results may differ from a plain program's by a relative error of at most 0.012.
The roundings to bfloat16 on the way count: a program that leaves them out, or rounds other values in their place, can miss the bound.
Values may be sent and summed in bfloat16 or wider, within the bound.
A program may use at most 64 MiB of HBM per device.

v0:
```python
import jax
import jax.numpy as jnp
from jax import lax
from jax.sharding import PartitionSpec as P

D = 2048
HEAD_SIZE = 128
QUERY_HEADS = 8
KEY_VALUE_HEADS = 2
GRID = 64
eps = 1e-06
rotary_base = 10000.0


def sent_together(arrays, axis, dim, along):
    ends, at = ([], 0)
    for a in arrays[:-1]:
        at += a.shape[along]
        ends.append(at)
    both = jnp.concatenate(arrays, axis=along)
    return tuple(jnp.split(lax.all_gather(both, axis, axis=dim, tiled=True), ends, axis=along))


def laid_out(tiles, dim):
    tiles = jnp.moveaxis(tiles, 0, dim)
    lengths = tiles.shape
    return tiles.reshape(*lengths[:dim], lengths[dim] * lengths[dim + 1], *lengths[dim + 2 :])


def sent_to_all(x, axis):
    size = lax.axis_size(axis)
    return lax.all_to_all(jnp.broadcast_to(x[None], (size, *x.shape)), axis, 0, 0, tiled=True)


def gathered_copies(x, axis, dim):
    return laid_out(sent_to_all(x, axis), dim)


def taken_together(x, axis):
    everything = sent_to_all(x, axis)
    return jnp.sum(everything, axis=0)


def in_blocks(x, dim, size):
    lengths = x.shape
    tiles = x.reshape(*lengths[:dim], size, lengths[dim] // size, *lengths[dim + 1 :])
    return jnp.moveaxis(tiles, dim, 0)


def summed_on_arrival(x, axis, dim):
    tiles = in_blocks(x, dim, lax.axis_size(axis))
    arrived = lax.all_to_all(tiles, axis, split_axis=0, concat_axis=0, tiled=True)
    return arrived.astype(jnp.float32).sum(axis=0)


def apply_rotary(vectors, grid_positions):
    half_size = vectors.shape[-1] // 2
    frequency = rotary_base ** (-jnp.arange(0, half_size, 2, dtype=jnp.float32) / half_size)
    grid_row = (grid_positions // GRID).astype(jnp.float32)
    grid_col = (grid_positions % GRID).astype(jnp.float32)
    angles = jnp.concatenate(
        [grid_row[:, None] * frequency, grid_col[:, None] * frequency], axis=-1
    )[:, None, :]
    cosine_table = jnp.cos(angles)
    sine_table = jnp.sin(angles)
    first_half = vectors[..., :half_size]
    second_half = vectors[..., half_size:]
    return jnp.concatenate(
        [
            first_half * cosine_table - second_half * sine_table,
            first_half * sine_table + second_half * cosine_table,
        ],
        axis=-1,
    )


def per_head_norm(vectors, gain):
    return vectors * lax.rsqrt(jnp.mean(vectors * vectors, axis=-1, keepdims=True) + eps) * gain


def on_device(
    residual_in,
    queries,
    keys,
    values,
    query_gain,
    key_norm_gain,
    out_weight,
    mlp_gain,
    gate_weight,
    up_weight,
    down_weight,
):
    local_rows = residual_in.shape[0]
    local_heads = queries.shape[1] // HEAD_SIZE
    queries_per_group = QUERY_HEADS // KEY_VALUE_HEADS
    tp_index = lax.axis_index("tp")
    tp_count = lax.axis_size("tp")
    grid_positions = lax.axis_index("sp") * local_rows + jnp.arange(local_rows, dtype=jnp.int32)
    weight_cols = lax.all_to_all(out_weight, "tp", split_axis=1, concat_axis=0, tiled=True)
    query_rows = apply_rotary(
        per_head_norm(
            queries.astype(jnp.float32).reshape(local_rows, local_heads, HEAD_SIZE), query_gain
        ),
        grid_positions,
    ).astype(jnp.bfloat16)
    query_matrix = jnp.transpose(query_rows, (1, 0, 2)).reshape(local_heads * local_rows, HEAD_SIZE)
    shared = tp_index * local_heads // queries_per_group
    own_keys = lax.dynamic_slice_in_dim(keys, shared * HEAD_SIZE, HEAD_SIZE, 1)
    own_values = lax.dynamic_slice_in_dim(values, shared * HEAD_SIZE, HEAD_SIZE, 1)
    key_matrix = apply_rotary(
        per_head_norm(own_keys.astype(jnp.float32)[:, None, :], key_norm_gain), grid_positions
    )[:, 0, :].astype(jnp.bfloat16)
    score_scale = HEAD_SIZE ** (-0.5)
    query_count = local_heads * local_rows
    start_state = (
        jnp.full((query_count,), -1e30, jnp.float32),
        jnp.zeros((query_count,), jnp.float32),
        jnp.zeros((query_count, HEAD_SIZE), jnp.float32),
    )
    key_piece, value_piece = sent_together((key_matrix, own_values), "sp", 0, 1)
    piece_rows = key_piece.shape[0]
    block_count = -(-piece_rows // 2048)
    while piece_rows % block_count:
        block_count += 1
    block_width = piece_rows // block_count

    def one_block(block_index, state_inner):
        running_max, running_sum, weighted = state_inner
        block_keys = lax.dynamic_slice_in_dim(key_piece, block_index * block_width, block_width, 0)
        block_values = lax.dynamic_slice_in_dim(
            value_piece, block_index * block_width, block_width, 0
        )
        scores = (
            jnp.dot(query_matrix, block_keys.T, preferred_element_type=jnp.float32) * score_scale
        )
        new_max = jnp.maximum(running_max, jnp.max(scores, axis=1))
        factor = jnp.exp(running_max - new_max)
        weights = jnp.exp(scores - new_max[:, None])
        running_sum = running_sum * factor + jnp.sum(weights, axis=1)
        weighted = weighted * factor[:, None] + jnp.dot(
            weights.astype(jnp.bfloat16), block_values, preferred_element_type=jnp.float32
        )
        return (new_max, running_sum, weighted)

    running_max, running_sum, weighted = lax.fori_loop(0, block_count, one_block, start_state)
    attended = (weighted / running_sum[:, None]).astype(jnp.bfloat16)
    attended = jnp.transpose(
        attended.reshape(local_heads, local_rows, HEAD_SIZE), (1, 0, 2)
    ).reshape(local_rows, local_heads * HEAD_SIZE)
    own_width = residual_in.shape[1]
    attended_full = gathered_copies(attended, "tp", 1)
    group_width = local_heads * HEAD_SIZE
    share = jnp.zeros((local_rows, own_width), jnp.float32)
    for group_index in range(tp_count):
        left_part = attended_full[:, group_index * group_width : (group_index + 1) * group_width]
        right_part = weight_cols[group_index * group_width : (group_index + 1) * group_width, :]
        term = jnp.dot(left_part, right_part, preferred_element_type=jnp.float32).astype(
            jnp.bfloat16
        )
        share = share + term.astype(jnp.float32)
    residual_mid = residual_in.astype(jnp.float32) + share
    squares = taken_together(jnp.sum(residual_mid * residual_mid, axis=1), "tp")
    gain_own = lax.dynamic_slice_in_dim(mlp_gain, tp_index * own_width, own_width, 0)
    normed_own = (residual_mid * lax.rsqrt(squares / D + eps)[:, None] * gain_own).astype(
        jnp.bfloat16
    )
    normed = lax.all_gather(normed_own, "tp", axis=1, tiled=True)
    pieces = sent_together((gate_weight, up_weight), "sp", 0, 1)
    gate_out = jnp.dot(normed, pieces[0], preferred_element_type=jnp.float32)
    up_out = jnp.dot(normed, pieces[1], preferred_element_type=jnp.float32)
    hidden = (jax.nn.silu(gate_out) * up_out).astype(jnp.bfloat16)
    down_terms = jnp.dot(
        hidden,
        lax.all_gather(down_weight, "sp", axis=1, tiled=True),
        preferred_element_type=jnp.float32,
    )
    down_share = summed_on_arrival(down_terms.astype(jnp.bfloat16), "tp", 1)
    return (residual_mid + 0.5 * down_share).astype(jnp.bfloat16)


def solution(mesh):
    in_specs = (
        P("sp", "tp"),
        P("sp", "tp"),
        P("sp", None),
        P("sp", None),
        P(),
        P(),
        P("tp", None),
        P(),
        P("sp", "tp"),
        P("sp", "tp"),
        P("tp", "sp"),
    )
    out_specs = P("sp", "tp")
    return jax.shard_map(
        on_device, mesh=mesh, in_specs=in_specs, out_specs=out_specs, check_vma=False
    )
```

profile of v0, /device:TPU:1, one launch (start us, length us, event | category | flops | bytes accessed | tf_op | source)
XLA Modules:
  0.0 336.8 jit_solution(7837900333065985362)
XLA Ops:
  6.6 1.1 fusion.38
  7.7 1.1 fusion.41
  8.9 0.3 multiply_bitcast_fusion.1
  9.2 1.3 fusion.40
  10.5 1.8 fusion.44
  12.3 0.3 subtract_convert_fusion.1
  12.8 0.8 pad_maximum_fusion.1
  13.6 1.0 copy.61
  14.6 5.8 %all-to-all-start.1 = ((bf16[128,8,256]{0,2,1:T(8,128)(2,1)}), bf16[128,8,256]{0,2,1:T(8,128)(2,1)S(1)}, u32[]{:S(2)}, u32[]{:S(2)}) async-start(bf16[128,8,256]{0,2,1:T(8,128)(2,1)} %bitcast.9), calls=%async_computation.1 | async-start | bytes 1048576 | tf_op jit(solution)/shard_map/all_to_all | solution.py:100
  20.4 0.8 pad_maximum_fusion.2
  21.4 56.8 %all-gather.5.cloned.1.call-done = bf16[12288,256]{1,0:T(8,128)(2,1)} async-done(((bf16[768,256]{1,0:T(8,128)(2,1)}), bf16[12288,256]{1,0:T(8,128)(2,1)}) %all-gather.5.cloned.1.call-update) | async-done | bytes 6291472 | tf_op jit(solution)/shard_map/all_gather | solution.py:21
  78.2 4.7 %fusion.66 = (bf16[12288,128]{1,0:T(8,128)(2,1)}, bf16[12288,128]{1,0:T(8,128)(2,1)}) fusion(bf16[12288,256]{1,0:T(8,128)(2,1)} %all-gather.5.cloned.1.call-done), kind=kLoop, calls=%fused_computation.114 | loop fusion | bytes 12582912 | tf_op jit(solution)/shard_map/split | solution.py:21
  82.9 71.6 %while.18 = (s32[]{:T(128)}, f32[768]{0:T(1024)S(1)}, f32[768]{0:T(1024)S(1)}, f32[768,128]{1,0:T(8,128)S(1)}, bf16[12288,128]{1,0:T(8,128)(2,1)}, /*index=5*/bf...) while((s32[]{:T(128)}, f32[768]{0:T(1024)S(1)}, ...), condition=%wide.region_5.6_spmd.clone, body=%wide.region_2.5_spmd.clone.sunk | while | flops 818188032 | bytes 46121160 | solution.py:146
  82.9 4.7 %multiply_reduce_fusion.3 = (f32[768]{0:T(1024)S(1)}, f32[2048,768]{1,0:T(8,128)}) fusion(bf16[768,128]{1,0:T(8,128)(2,1)S(1)} %get-tuple-element.268, bf16[12288,128]{1,0:T(8,128)(2,1)} %get-tuple-element.267, s32[]{:T(128)S(6)} %select_n.55), kind=kOutput, calls=%fused_computation.1.clone.1 | convolution fusion | flops 405798144 | bytes 7015428 | tf_op jit(solution)/shard_map/while/body/eval_jaxpr/dot_general | solution.py:135
  87.6 4.2 %fusion.80 = f32[768]{0:T(1024)S(1)} fusion(f32[2048,768]{1,0:T(8,128)} %get-tuple-element.238, f32[768]{0:T(1024)S(1)} %select_maximum_fusion.2), kind=kLoop, calls=%fused_computation.3.clone.1 | loop fusion | flops 4717824 | bytes 6297600 | tf_op jit(solution)/shard_map/while/body/eval_jaxpr/reduce_sum | solution.py:140
  91.8 0.8 copy-done.1
  92.6 2.4 fusion.82
  95.0 4.7 %multiply_reduce_fusion.3 = (f32[768]{0:T(1024)S(1)}, f32[2048,768]{1,0:T(8,128)}) fusion(bf16[768,128]{1,0:T(8,128)(2,1)S(1)} %get-tuple-element.268, bf16[12288,128]{1,0:T(8,128)(2,1)} %get-tuple-element.267, s32[]{:T(128)S(6)} %select_n.55), kind=kOutput, calls=%fused_computation.1.clone.1 | convolution fusion | flops 405798144 | bytes 7015428 | tf_op jit(solution)/shard_map/while/body/eval_jaxpr/dot_general | solution.py:135
  99.6 4.1 %fusion.80 = f32[768]{0:T(1024)S(1)} fusion(f32[2048,768]{1,0:T(8,128)} %get-tuple-element.238, f32[768]{0:T(1024)S(1)} %select_maximum_fusion.2), kind=kLoop, calls=%fused_computation.3.clone.1 | loop fusion | flops 4717824 | bytes 6297600 | tf_op jit(solution)/shard_map/while/body/eval_jaxpr/reduce_sum | solution.py:140
  103.7 0.6 copy-done.1
  104.3 2.4 fusion.82
  106.7 4.7 %multiply_reduce_fusion.3 = (f32[768]{0:T(1024)S(1)}, f32[2048,768]{1,0:T(8,128)}) fusion(bf16[768,128]{1,0:T(8,128)(2,1)S(1)} %get-tuple-element.268, bf16[12288,128]{1,0:T(8,128)(2,1)} %get-tuple-element.267, s32[]{:T(128)S(6)} %select_n.55), kind=kOutput, calls=%fused_computation.1.clone.1 | convolution fusion | flops 405798144 | bytes 7015428 | tf_op jit(solution)/shard_map/while/body/eval_jaxpr/dot_general | solution.py:135
  111.4 4.2 %fusion.80 = f32[768]{0:T(1024)S(1)} fusion(f32[2048,768]{1,0:T(8,128)} %get-tuple-element.238, f32[768]{0:T(1024)S(1)} %select_maximum_fusion.2), kind=kLoop, calls=%fused_computation.3.clone.1 | loop fusion | flops 4717824 | bytes 6297600 | tf_op jit(solution)/shard_map/while/body/eval_jaxpr/reduce_sum | solution.py:140
  115.6 0.8 copy-done.1
  116.4 2.4 fusion.82
  118.8 4.7 %multiply_reduce_fusion.3 = (f32[768]{0:T(1024)S(1)}, f32[2048,768]{1,0:T(8,128)}) fusion(bf16[768,128]{1,0:T(8,128)(2,1)S(1)} %get-tuple-element.268, bf16[12288,128]{1,0:T(8,128)(2,1)} %get-tuple-element.267, s32[]{:T(128)S(6)} %select_n.55), kind=kOutput, calls=%fused_computation.1.clone.1 | convolution fusion | flops 405798144 | bytes 7015428 | tf_op jit(solution)/shard_map/while/body/eval_jaxpr/dot_general | solution.py:135
  123.5 4.2 %fusion.80 = f32[768]{0:T(1024)S(1)} fusion(f32[2048,768]{1,0:T(8,128)} %get-tuple-element.238, f32[768]{0:T(1024)S(1)} %select_maximum_fusion.2), kind=kLoop, calls=%fused_computation.3.clone.1 | loop fusion | flops 4717824 | bytes 6297600 | tf_op jit(solution)/shard_map/while/body/eval_jaxpr/reduce_sum | solution.py:140
  127.7 0.8 copy-done.1
  128.5 2.4 fusion.82
  130.9 4.7 %multiply_reduce_fusion.3 = (f32[768]{0:T(1024)S(1)}, f32[2048,768]{1,0:T(8,128)}) fusion(bf16[768,128]{1,0:T(8,128)(2,1)S(1)} %get-tuple-element.268, bf16[12288,128]{1,0:T(8,128)(2,1)} %get-tuple-element.267, s32[]{:T(128)S(6)} %select_n.55), kind=kOutput, calls=%fused_computation.1.clone.1 | convolution fusion | flops 405798144 | bytes 7015428 | tf_op jit(solution)/shard_map/while/body/eval_jaxpr/dot_general | solution.py:135
  135.6 4.2 %fusion.80 = f32[768]{0:T(1024)S(1)} fusion(f32[2048,768]{1,0:T(8,128)} %get-tuple-element.238, f32[768]{0:T(1024)S(1)} %select_maximum_fusion.2), kind=kLoop, calls=%fused_computation.3.clone.1 | loop fusion | flops 4717824 | bytes 6297600 | tf_op jit(solution)/shard_map/while/body/eval_jaxpr/reduce_sum | solution.py:140
  139.8 0.7 copy-done.1
  140.5 2.4 fusion.82
  142.9 4.7 %multiply_reduce_fusion.3 = (f32[768]{0:T(1024)S(1)}, f32[2048,768]{1,0:T(8,128)}) fusion(bf16[768,128]{1,0:T(8,128)(2,1)S(1)} %get-tuple-element.268, bf16[12288,128]{1,0:T(8,128)(2,1)} %get-tuple-element.267, s32[]{:T(128)S(6)} %select_n.55), kind=kOutput, calls=%fused_computation.1.clone.1 | convolution fusion | flops 405798144 | bytes 7015428 | tf_op jit(solution)/shard_map/while/body/eval_jaxpr/dot_general | solution.py:135
  147.5 4.0 %fusion.80 = f32[768]{0:T(1024)S(1)} fusion(f32[2048,768]{1,0:T(8,128)} %get-tuple-element.238, f32[768]{0:T(1024)S(1)} %select_maximum_fusion.2), kind=kLoop, calls=%fused_computation.3.clone.1 | loop fusion | flops 4717824 | bytes 6297600 | tf_op jit(solution)/shard_map/while/body/eval_jaxpr/reduce_sum | solution.py:140
  151.6 0.6 copy-done.1
  152.1 2.4 fusion.82
  154.9 1.3 broadcast_in_dim.17
  156.2 5.2 %all-to-all-start = ((bf16[8,768,128]{1,2,0:T(8,128)(2,1)}), bf16[8,768,128]{1,2,0:T(8,128)(2,1)S(1)}, u32[]{:S(2)}, u32[]{:S(2)}) async-start(bf16[8,768,128]{1,2,0:T(8,128)(2,1)} %broadcast_in_dim.17), calls=%async_computation | async-start | bytes 3145728 | tf_op jit(solution)/shard_map/all_to_all | solution.py:32
  161.4 1.9 copy.59
  163.3 18.7 %all-to-all-done = bf16[8,768,128]{1,2,0:T(8,128)(2,1)S(1)} async-done(((bf16[8,768,128]{1,2,0:T(8,128)(2,1)}), bf16[8,768,128]{1,2,0:T(8,128)(2,1)S(1)}, u32[]{:S(2)}, u32[]{:S(2)}) %all-to-all-start) | async-done | bytes 1572896 | tf_op jit(solution)/shard_map/all_to_all | solution.py:32
  182.0 0.2 fusion.35
  182.2 0.2 fusion.34
  182.5 0.2 fusion.32
  182.7 0.2 fusion.30
  183.0 0.2 fusion.28
  183.2 0.2 fusion.26
  183.5 0.2 fusion.24
  184.0 0.3 multiply_reduce_fusion.1
  184.3 0.6 broadcast_in_dim.18
  184.9 4.2 %all-to-all-start.2 = ((f32[8,1,768]{2,1,0:T(1,128)}), f32[8,1,768]{2,1,0:T(1,128)S(1)}, u32[]{:S(2)}, u32[]{:S(2)}) async-start(f32[8,1,768]{2,1,0:T(1,128)} %broadcast_in_dim.18), calls=%async_computation.2 | async-start | bytes 49152 | tf_op jit(solution)/shard_map/all_to_all | solution.py:32
  189.1 0.8 dynamic_slice.25
  189.9 3.9 %all-to-all-done.2 = f32[8,1,768]{2,1,0:T(1,128)S(1)} async-done(((f32[8,1,768]{2,1,0:T(1,128)}), f32[8,1,768]{2,1,0:T(1,128)S(1)}, u32[]{:S(2)}, u32[]{:S(2)}) %all-to-all-start.2) | async-done | bytes 24608 | tf_op jit(solution)/shard_map/all_to_all | solution.py:32
  193.9 0.9 multiply_convert_fusion.1
  195.0 0.3 all-gather.11.cloned.1.call-update
  195.3 24.9 %all-gather.7.cloned.1.call-done = bf16[768,2048]{0,1:T(8,128)(2,1)} async-done(((bf16[768,256]{0,1:T(8,128)(2,1)}), bf16[768,2048]{0,1:T(8,128)(2,1)}) %all-gather.7.cloned.1.call-update) | async-done | bytes 3145744 | tf_op jit(solution)/shard_map/all_gather | solution.py:168
  220.2 5.2 %fusion.16 = f32[768,704]{0,1:T(8,128)S(1)} fusion(bf16[768,2048]{0,1:T(8,128)(2,1)} %all-gather.7.cloned.1.call-done, bf16[2048,1408]{0,1:T(8,128)(2,1)} %all-gather.9.cloned.1.call-done), kind=kOutput, calls=%fused_computation.22 | convolution fusion | flops 2214592512 | bytes 8192000 | tf_op jit(solution)/shard_map/dot_general | solution.py:170
  225.4 45.8 %all-gather.11.cloned.1.call-done = bf16[704,2048]{1,0:T(8,128)(2,1)} async-done(((bf16[704,128]{1,0:T(8,128)(2,1)}), bf16[704,2048]{1,0:T(8,128)(2,1)}) %all-gather.11.cloned.1.call-update) | async-done | bytes 2883600 | tf_op jit(solution)/shard_map/all_gather | solution.py:175
  271.2 11.7 %convolution_convert_fusion = bf16[768,2048]{1,0:T(8,128)(2,1)} fusion(bf16[704,2048]{1,0:T(8,128)(2,1)} %all-gather.11.cloned.1.call-done, f32[768,704]{0,1:T(8,128)S(1)} %fusion.16, bf16[768,2048]{0,1:T(8,128)(2,1)} %all-gather.7.cloned.1.call-done, bf16[2048,1408]{0,1:T(8,128)(2,1)} %all-gather.9.cloned.1.call-done), kind=kOutput, calls=%fused_computation.18 | convolution fusion | flops 4434001920 | bytes 14221312 | tf_op jit(solution)/shard_map/dot_general | solution.py:173
  282.9 2.1 copy.79
  285.0 43.5 %all_to_all.32 = bf16[8,768,256]{2,1,0:T(8,128)(2,1)S(1)} all-to-all(bf16[8,768,256]{2,1,0:T(8,128)(2,1)S(1)} %bitcast.66), channel_id=1, replica_groups=mesh['sp'=16,'tp'=8] {'tp'}, dimensions={0} | all-to-all | bytes 6291456 | tf_op jit(solution)/shard_map/all_to_all | solution.py:52
  328.5 0.4 convert_reduce_fusion
  329.0 0.3 copy.73
  329.3 0.9 copy.74
  (58 shorter events, 1.4 us)
Async XLA Ops:
  6.5 2.4 copy-start
  6.5 71.7 %all-gather.5.cloned.1.call-start = ((), (), s32[]{:S(2)}) async-start(), calls=%async_computation.4 | async-start | bytes 6684672 | tf_op jit(solution)/shard_map/all_gather | solution.py:21
  10.5 3.1 copy-start.3
  12.3 8.1 %copy-start.4 = (bf16[128,704]{0,1:T(8,128)(2,1)S(1)}, bf16[128,704]{0,1:T(8,128)(2,1)}, u32[]{:S(2)}) copy-start(bf16[128,704]{0,1:T(8,128)(2,1)} %param.22) | copy-start | bytes 540676
  12.3 8.1 %copy-start.5 = (bf16[128,704]{0,1:T(8,128)(2,1)S(1)}, bf16[128,704]{0,1:T(8,128)(2,1)}, u32[]{:S(2)}) copy-start(bf16[128,704]{0,1:T(8,128)(2,1)} %param.21) | copy-start | bytes 540676
  14.6 140.2 %all-to-all-start.1 = ((bf16[128,8,256]{0,2,1:T(8,128)(2,1)}), bf16[128,8,256]{0,2,1:T(8,128)(2,1)S(1)}, u32[]{:S(2)}, u32[]{:S(2)}) async-start(bf16[128,8,256]{0,2,1:T(8,128)(2,1)} %bitcast.9), calls=%async_computation.1 | async-start | bytes 1048576 | tf_op jit(solution)/shard_map/all_to_all | solution.py:100
  20.4 174.9 %all-gather.9.cloned.1.call-start = ((), (), s32[]{:S(2)}) async-start(), calls=%async_computation.6 | async-start | bytes 6127616 | tf_op jit(solution)/shard_map/all_gather | solution.py:21
  87.6 5.0 %copy-start.1 = (f32[2048,768]{1,0:T(8,128)S(1)}, f32[2048,768]{1,0:T(8,128)}, u32[]{:S(2)}) copy-start(f32[2048,768]{1,0:T(8,128)} %get-tuple-element.238) | copy-start | bytes 18874372 | tf_op jit(solution)/shard_map/while
  99.6 4.7 %copy-start.1 = (f32[2048,768]{1,0:T(8,128)S(1)}, f32[2048,768]{1,0:T(8,128)}, u32[]{:S(2)}) copy-start(f32[2048,768]{1,0:T(8,128)} %get-tuple-element.238) | copy-start | bytes 18874372 | tf_op jit(solution)/shard_map/while
  111.4 5.0 %copy-start.1 = (f32[2048,768]{1,0:T(8,128)S(1)}, f32[2048,768]{1,0:T(8,128)}, u32[]{:S(2)}) copy-start(f32[2048,768]{1,0:T(8,128)} %get-tuple-element.238) | copy-start | bytes 18874372 | tf_op jit(solution)/shard_map/while
  123.5 5.0 %copy-start.1 = (f32[2048,768]{1,0:T(8,128)S(1)}, f32[2048,768]{1,0:T(8,128)}, u32[]{:S(2)}) copy-start(f32[2048,768]{1,0:T(8,128)} %get-tuple-element.238) | copy-start | bytes 18874372 | tf_op jit(solution)/shard_map/while
  135.6 4.9 %copy-start.1 = (f32[2048,768]{1,0:T(8,128)S(1)}, f32[2048,768]{1,0:T(8,128)}, u32[]{:S(2)}) copy-start(f32[2048,768]{1,0:T(8,128)} %get-tuple-element.238) | copy-start | bytes 18874372 | tf_op jit(solution)/shard_map/while
  147.5 4.6 %copy-start.1 = (f32[2048,768]{1,0:T(8,128)S(1)}, f32[2048,768]{1,0:T(8,128)}, u32[]{:S(2)}) copy-start(f32[2048,768]{1,0:T(8,128)} %get-tuple-element.238) | copy-start | bytes 18874372 | tf_op jit(solution)/shard_map/while
  156.2 25.8 %all-to-all-start = ((bf16[8,768,128]{1,2,0:T(8,128)(2,1)}), bf16[8,768,128]{1,2,0:T(8,128)(2,1)S(1)}, u32[]{:S(2)}, u32[]{:S(2)}) async-start(bf16[8,768,128]{1,2,0:T(8,128)(2,1)} %broadcast_in_dim.17), calls=%async_computation | async-start | bytes 3145728 | tf_op jit(solution)/shard_map/all_to_all | solution.py:32
  183.0 1.0 copy-start.2
  184.9 8.9 %all-to-all-start.2 = ((f32[8,1,768]{2,1,0:T(1,128)}), f32[8,1,768]{2,1,0:T(1,128)S(1)}, u32[]{:S(2)}, u32[]{:S(2)}) async-start(f32[8,1,768]{2,1,0:T(1,128)} %broadcast_in_dim.18), calls=%async_computation.2 | async-start | bytes 49152 | tf_op jit(solution)/shard_map/all_to_all | solution.py:32
  189.1 31.1 %all-gather.7.cloned.1.call-start = ((), (), s32[]{:S(2)}) async-start(), calls=%async_computation.5 | async-start | bytes 3538944 | tf_op jit(solution)/shard_map/all_gather | solution.py:168
  194.7 76.4 %all-gather.11.cloned.1.call-start = ((), (), s32[]{:S(2)}) async-start(), calls=%async_computation.7 | async-start | bytes 3063808 | tf_op jit(solution)/shard_map/all_gather | solution.py:175
Sparse Core Ops, SparseCore 0:
  13.7 64.4 all-gather.4
  80.3 62.8 all-gather.8
  194.9 25.3 all-gather.6
  222.2 48.9 all-gather.10
where the time goes:
time: 338 us; the launch traced here: 337 us
  waiting for transfers between devices  151 us (45%)
  matrix products  61.1 us (18%)
  blocking collectives  43.5 us (13%)
  other arithmetic  34.3 us (10%)
  local copies, waits for them, and re-layouts  18.2 us (5%)
  starting transfers between devices  15.5 us (5%)
  between operations  13.4 us (4%)
    all_gather x2, waiting for transfers between devices, sent_together(): lax.all_gather(both, axis, axis=dim, tiled=True)  56.8 us
    all_gather x1, waiting for transfers between devices, on_device(): lax.all_gather(down_weight, 'sp', axis=1, tiled=True)  45.8 us
    all_to_all x1, blocking collectives, summed_on_arrival(): lax.all_to_all(tiles, axis, split_axis=0, concat_axis=0, tiled=True)  43.5 us
    dot_general x6, matrix products, one_block(): jnp.dot(query_matrix, block_keys.T, preferred_element_type=jnp.float32)  28 us
    all_gather x1, waiting for transfers between devices, on_device(): normed = lax.all_gather(normed_own, 'tp', axis=1, tiled=True)  24.9 us
    reduce_sum x6, other arithmetic, one_block(): running_sum = running_sum * factor + jnp.sum(weights, axis=1)  24.8 us
    all_to_all x2, waiting for transfers between devices, sent_to_all(): lax.all_to_all(jnp.broadcast_to(x[None], (size, *x.shape)), axis, 0, 0, t...  22.6 us
    dot_general x6, matrix products, one_block(): jnp.dot(weights.astype(jnp.bfloat16), block_values, preferred_element_typ...  14.2 us
  transfers between devices with their start and end apart: 7, of which 5 were waited for; matrix products, arithmetic and copies ran while one was open for 26% of the time, Pallas kernels for 0%

commit v1 on v0

--- a/solution.py
+++ b/solution.py
@@ -10,6 +10,14 @@
 GRID = 64
 eps = 1e-06
 rotary_base = 10000.0
+
+
+def gather_by_exchange(shard, axis, dim):
+    count = lax.axis_size(axis)
+    repeats = [count if d == dim else 1 for d in range(shard.ndim)]
+    return lax.all_to_all(
+        jnp.tile(shard, repeats), axis, split_axis=dim, concat_axis=dim, tiled=True
+    )
 
 
 def sent_together(arrays, axis, dim, along):
@@ -165,7 +173,7 @@
     normed_own = (residual_mid * lax.rsqrt(squares / D + eps)[:, None] * gain_own).astype(
         jnp.bfloat16
     )
-    normed = lax.all_gather(normed_own, "tp", axis=1, tiled=True)
+    normed = gather_by_exchange(normed_own, "tp", 1)
     pieces = sent_together((gate_weight, up_weight), "sp", 0, 1)
     gate_out = jnp.dot(normed, pieces[0], preferred_element_type=jnp.float32)
     up_out = jnp.dot(normed, pieces[1], preferred_element_type=jnp.float32)

time: 338 us -> 308 us (0.911)
  waiting for transfers between devices: 151 us -> 80.5 us
  blocking collectives: 43.5 us -> 81.6 us
    all_gather x1, waiting for transfers between devices: 45.8 us -> 0.01 us  [on_device(): lax.all_gather(down_weight, 'sp', axis=1, tiled=True)]
    all_to_all x0 -> x1, blocking collectives: none -> 40.5 us  [gather_by_exchange(): lax.all_to_all(jnp.tile(shard, repeats), axis, split_axis=dim, concat_axi...]
    all_gather x1 -> x0, waiting for transfers between devices: 24.9 us -> none  [on_device(): normed = lax.all_gather(normed_own, 'tp', axis=1, tiled=True)]
    dot_general x8, matrix products: 1.99 us -> 8.71 us  [on_device(): jnp.dot(left_part, right_part, preferred_element_type=jnp.float32)]
    dot_general x6, matrix products: 14.2 us -> 7.94 us  [one_block(): jnp.dot(weights.astype(jnp.bfloat16), block_values, preferred_element_typ...]
  transfers between devices with their start and end apart: 7 -> 6, of which waited for: 5 -> 3; matrix products, arithmetic and copies ran while one was open for 26% -> 29% of each run, Pallas kernels for 0% -> 0%
where the time goes in v1:
time: 308 us; the launch traced here: 307 us
  blocking collectives  81.6 us (26%)
  waiting for transfers between devices  80.5 us (26%)
  matrix products  63.2 us (21%)
  other arithmetic  33.7 us (11%)
  local copies, waits for them, and re-layouts  19 us (6%)
  starting transfers between devices  15.1 us (5%)
  between operations  13.4 us (4%)
    all_gather x2, waiting for transfers between devices, sent_together(): lax.all_gather(both, axis, axis=dim, tiled=True)  56.1 us
    all_to_all x1, blocking collectives, summed_on_arrival(): lax.all_to_all(tiles, axis, split_axis=0, concat_axis=0, tiled=True)  41 us
    all_to_all x1, blocking collectives, gather_by_exchange(): lax.all_to_all(jnp.tile(shard, repeats), axis, split_axis=dim, concat_axi...  40.5 us
    dot_general x6, matrix products, one_block(): jnp.dot(query_matrix, block_keys.T, preferred_element_type=jnp.float32)  28.4 us
    reduce_sum x6, other arithmetic, one_block(): running_sum = running_sum * factor + jnp.sum(weights, axis=1)  24.2 us
    all_to_all x2, waiting for transfers between devices, sent_to_all(): lax.all_to_all(jnp.broadcast_to(x[None], (size, *x.shape)), axis, 0, 0, t...  23.7 us
    dot_general x1, matrix products, on_device(): jnp.dot(hidden, lax.all_gather(down_weight, 'sp', axis=1, tiled=True), pr...  11.5 us
    all_to_all x2, starting transfers between devices, sent_to_all(): lax.all_to_all(jnp.broadcast_to(x[None], (size, *x.shape)), axis, 0, 0, t...  9.3 us
  transfers between devices with their start and end apart: 6, of which 3 were waited for; matrix products, arithmetic and copies ran while one was open for 29% of the time, Pallas kernels for 0%

profile of v1, /device:TPU:1, one launch (start us, length us, event | category | flops | bytes accessed | tf_op | source)
XLA Modules:
  0.0 306.6 jit_solution(2725025384899518010)
XLA Ops:
  6.6 1.1 fusion.38
  7.7 1.1 fusion.41
  8.9 0.3 multiply_bitcast_fusion.1
  9.2 1.3 fusion.40
  10.5 1.8 fusion.44
  12.3 0.3 subtract_convert_fusion.1
  12.8 0.8 pad_maximum_fusion.1
  13.6 1.0 copy.84
  14.7 5.8 %all-to-all-start.1 = ((bf16[128,8,256]{0,2,1:T(8,128)(2,1)}), bf16[128,8,256]{0,2,1:T(8,128)(2,1)}, u32[]{:S(2)}, u32[]{:S(2)}) async-start(bf16[128,8,256]{0,2,1:T(8,128)(2,1)} %bitcast.9), calls=%async_computation.1 | async-start | bytes 1048576 | tf_op jit(solution)/shard_map/all_to_all | solution.py:108
  20.5 0.8 pad_maximum_fusion.2
  21.3 0.8 pad_maximum_fusion.3
  22.1 56.1 %all-gather.4.cloned.1.call-done = bf16[12288,256]{1,0:T(8,128)(2,1)} async-done(((bf16[768,256]{1,0:T(8,128)(2,1)}), bf16[12288,256]{1,0:T(8,128)(2,1)}) %all-gather.4.cloned.1.call-update) | async-done | bytes 6291472 | tf_op jit(solution)/shard_map/all_gather | solution.py:29
  78.2 4.2 %fusion.66 = (bf16[12288,128]{1,0:T(8,128)(2,1)S(1)}, bf16[12288,128]{1,0:T(8,128)(2,1)}) fusion(bf16[12288,256]{1,0:T(8,128)(2,1)} %all-gather.4.cloned.1.call-done), kind=kLoop, calls=%fused_computation.114 | loop fusion | bytes 12582912 | tf_op jit(solution)/shard_map/split | solution.py:29
  82.4 64.6 %while.18 = (s32[]{:T(128)}, f32[768]{0:T(1024)S(1)}, f32[768]{0:T(1024)S(1)}, f32[768,128]{1,0:T(8,128)S(1)}, bf16[12288,128]{1,0:T(8,128)(2,1)}, /*index=5*/bf...) while((s32[]{:T(128)}, f32[768]{0:T(1024)S(1)}, ...), condition=%wide.region_5.6_spmd.clone, body=%wide.region_2.5_spmd.clone.sunk | while | flops 818188032 | bytes 46123208 | solution.py:154
  82.4 4.7 %multiply_reduce_fusion.3 = (f32[768]{0:T(1024)S(1)}, f32[2048,768]{1,0:T(8,128)}) fusion(bf16[768,128]{1,0:T(8,128)(2,1)} %get-tuple-element.268, bf16[12288,128]{1,0:T(8,128)(2,1)} %get-tuple-element.267, s32[]{:T(128)S(6)} %select_n.55), kind=kOutput, calls=%fused_computation.1.clone.1 | convolution fusion | flops 405798144 | bytes 7015428 | tf_op jit(solution)/shard_map/while/body/eval_jaxpr/dot_general | solution.py:143
  87.1 4.1 %fusion.80 = f32[768]{0:T(1024)S(1)} fusion(f32[2048,768]{1,0:T(8,128)} %get-tuple-element.238, f32[768]{0:T(1024)S(1)} %select_maximum_fusion.2), kind=kLoop, calls=%fused_computation.3.clone.1 | loop fusion | flops 4717824 | bytes 6297600 | tf_op jit(solution)/shard_map/while/body/eval_jaxpr/reduce_sum | solution.py:148
  91.2 0.8 copy-done.2
  92.0 1.3 fusion.82
  93.4 4.7 %multiply_reduce_fusion.3 = (f32[768]{0:T(1024)S(1)}, f32[2048,768]{1,0:T(8,128)}) fusion(bf16[768,128]{1,0:T(8,128)(2,1)} %get-tuple-element.268, bf16[12288,128]{1,0:T(8,128)(2,1)} %get-tuple-element.267, s32[]{:T(128)S(6)} %select_n.55), kind=kOutput, calls=%fused_computation.1.clone.1 | convolution fusion | flops 405798144 | bytes 7015428 | tf_op jit(solution)/shard_map/while/body/eval_jaxpr/dot_general | solution.py:143
  98.1 4.1 %fusion.80 = f32[768]{0:T(1024)S(1)} fusion(f32[2048,768]{1,0:T(8,128)} %get-tuple-element.238, f32[768]{0:T(1024)S(1)} %select_maximum_fusion.2), kind=kLoop, calls=%fused_computation.3.clone.1 | loop fusion | flops 4717824 | bytes 6297600 | tf_op jit(solution)/shard_map/while/body/eval_jaxpr/reduce_sum | solution.py:148
  102.2 0.6 copy-done.2
  102.8 1.3 fusion.82
  104.1 4.7 %multiply_reduce_fusion.3 = (f32[768]{0:T(1024)S(1)}, f32[2048,768]{1,0:T(8,128)}) fusion(bf16[768,128]{1,0:T(8,128)(2,1)} %get-tuple-element.268, bf16[12288,128]{1,0:T(8,128)(2,1)} %get-tuple-element.267, s32[]{:T(128)S(6)} %select_n.55), kind=kOutput, calls=%fused_computation.1.clone.1 | convolution fusion | flops 405798144 | bytes 7015428 | tf_op jit(solution)/shard_map/while/body/eval_jaxpr/dot_general | solution.py:143
  108.9 4.0 %fusion.80 = f32[768]{0:T(1024)S(1)} fusion(f32[2048,768]{1,0:T(8,128)} %get-tuple-element.238, f32[768]{0:T(1024)S(1)} %select_maximum_fusion.2), kind=kLoop, calls=%fused_computation.3.clone.1 | loop fusion | flops 4717824 | bytes 6297600 | tf_op jit(solution)/shard_map/while/body/eval_jaxpr/reduce_sum | solution.py:148
  112.9 0.6 copy-done.2
  113.5 1.3 fusion.82
  114.8 4.7 %multiply_reduce_fusion.3 = (f32[768]{0:T(1024)S(1)}, f32[2048,768]{1,0:T(8,128)}) fusion(bf16[768,128]{1,0:T(8,128)(2,1)} %get-tuple-element.268, bf16[12288,128]{1,0:T(8,128)(2,1)} %get-tuple-element.267, s32[]{:T(128)S(6)} %select_n.55), kind=kOutput, calls=%fused_computation.1.clone.1 | convolution fusion | flops 405798144 | bytes 7015428 | tf_op jit(solution)/shard_map/while/body/eval_jaxpr/dot_general | solution.py:143
  119.6 4.0 %fusion.80 = f32[768]{0:T(1024)S(1)} fusion(f32[2048,768]{1,0:T(8,128)} %get-tuple-element.238, f32[768]{0:T(1024)S(1)} %select_maximum_fusion.2), kind=kLoop, calls=%fused_computation.3.clone.1 | loop fusion | flops 4717824 | bytes 6297600 | tf_op jit(solution)/shard_map/while/body/eval_jaxpr/reduce_sum | solution.py:148
  123.6 0.6 copy-done.2
  124.2 1.3 fusion.82
  125.5 4.7 %multiply_reduce_fusion.3 = (f32[768]{0:T(1024)S(1)}, f32[2048,768]{1,0:T(8,128)}) fusion(bf16[768,128]{1,0:T(8,128)(2,1)} %get-tuple-element.268, bf16[12288,128]{1,0:T(8,128)(2,1)} %get-tuple-element.267, s32[]{:T(128)S(6)} %select_n.55), kind=kOutput, calls=%fused_computation.1.clone.1 | convolution fusion | flops 405798144 | bytes 7015428 | tf_op jit(solution)/shard_map/while/body/eval_jaxpr/dot_general | solution.py:143
  130.3 4.0 %fusion.80 = f32[768]{0:T(1024)S(1)} fusion(f32[2048,768]{1,0:T(8,128)} %get-tuple-element.238, f32[768]{0:T(1024)S(1)} %select_maximum_fusion.2), kind=kLoop, calls=%fused_computation.3.clone.1 | loop fusion | flops 4717824 | bytes 6297600 | tf_op jit(solution)/shard_map/while/body/eval_jaxpr/reduce_sum | solution.py:148
  134.3 0.6 copy-done.2
  134.9 1.3 fusion.82
  136.3 4.7 %multiply_reduce_fusion.3 = (f32[768]{0:T(1024)S(1)}, f32[2048,768]{1,0:T(8,128)}) fusion(bf16[768,128]{1,0:T(8,128)(2,1)} %get-tuple-element.268, bf16[12288,128]{1,0:T(8,128)(2,1)} %get-tuple-element.267, s32[]{:T(128)S(6)} %select_n.55), kind=kOutput, calls=%fused_computation.1.clone.1 | convolution fusion | flops 405798144 | bytes 7015428 | tf_op jit(solution)/shard_map/while/body/eval_jaxpr/dot_general | solution.py:143
  141.0 4.0 %fusion.80 = f32[768]{0:T(1024)S(1)} fusion(f32[2048,768]{1,0:T(8,128)} %get-tuple-element.238, f32[768]{0:T(1024)S(1)} %select_maximum_fusion.2), kind=kLoop, calls=%fused_computation.3.clone.1 | loop fusion | flops 4717824 | bytes 6297600 | tf_op jit(solution)/shard_map/while/body/eval_jaxpr/reduce_sum | solution.py:148
  145.1 0.6 copy-done.2
  145.6 1.3 fusion.82
  147.4 1.3 broadcast_in_dim.17
  148.6 5.1 %all-to-all-start = ((bf16[8,768,128]{1,2,0:T(8,128)(2,1)}), bf16[8,768,128]{1,2,0:T(8,128)(2,1)S(1)}, u32[]{:S(2)}, u32[]{:S(2)}) async-start(bf16[8,768,128]{1,2,0:T(8,128)(2,1)} %broadcast_in_dim.17), calls=%async_computation | async-start | bytes 3145728 | tf_op jit(solution)/shard_map/all_to_all | solution.py:40
  153.7 0.7 all-gather.8.cloned.1.call-update
  154.6 19.7 %all-to-all-done = bf16[8,768,128]{1,2,0:T(8,128)(2,1)S(1)} async-done(((bf16[8,768,128]{1,2,0:T(8,128)(2,1)}), bf16[8,768,128]{1,2,0:T(8,128)(2,1)S(1)}, u32[]{:S(2)}, u32[]{:S(2)}) %all-to-all-start) | async-done | bytes 1572896 | tf_op jit(solution)/shard_map/all_to_all | solution.py:40
  174.3 1.1 fusion.35
  175.4 1.1 fusion.34
  176.5 1.1 fusion.32
  177.6 1.1 fusion.30
  178.6 1.1 fusion.28
  179.7 1.1 fusion.26
  180.8 1.1 fusion.24
  181.9 1.1 multiply_reduce_fusion.1
  183.1 0.7 broadcast_in_dim.18
  183.7 4.2 %all-to-all-start.2 = ((f32[8,1,768]{2,1,0:T(1,128)}), f32[8,1,768]{2,1,0:T(1,128)S(1)}, u32[]{:S(2)}, u32[]{:S(2)}) async-start(f32[8,1,768]{2,1,0:T(1,128)} %broadcast_in_dim.18), calls=%async_computation.2 | async-start | bytes 49152 | tf_op jit(solution)/shard_map/all_to_all | solution.py:40
  188.0 0.8 dynamic_slice.25
  188.7 4.0 %all-to-all-done.2 = f32[8,1,768]{2,1,0:T(1,128)S(1)} async-done(((f32[8,1,768]{2,1,0:T(1,128)}), f32[8,1,768]{2,1,0:T(1,128)S(1)}, u32[]{:S(2)}, u32[]{:S(2)}) %all-to-all-start.2) | async-done | bytes 24608 | tf_op jit(solution)/shard_map/all_to_all | solution.py:40
  193.3 40.5 %all_to_all.41 = bf16[768,8,256]{2,0,1:T(8,128)(2,1)S(1)} all-to-all(bf16[768,8,256]{2,0,1:T(8,128)(2,1)S(1)} %tile.2), channel_id=1, replica_groups=mesh['sp'=16,'tp'=8] {'tp'}, dimensions={1} | all-to-all | bytes 6291456 | tf_op jit(solution)/shard_map/all_to_all | solution.py:18
  233.8 2.8 copy.95
  236.7 6.7 %fusion.16 = f32[768,704]{0,1:T(8,128)} fusion(bf16[768,2048]{0,1:T(8,128)(2,1)} %bitcast.76, bf16[2048,1408]{0,1:T(8,128)(2,1)} %all-gather.6.cloned.1.call-done), kind=kOutput, calls=%fused_computation.22 | convolution fusion | flops 2214592512 | bytes 8192000 | tf_op jit(solution)/shard_map/dot_general | solution.py:178
  243.4 11.5 %convolution_convert_fusion = bf16[768,2048]{1,0:T(8,128)(2,1)} fusion(bf16[704,2048]{1,0:T(8,128)(2,1)} %all-gather.8.cloned.1.call-done, f32[768,704]{0,1:T(8,128)} %fusion.16, bf16[768,2048]{0,1:T(8,128)(2,1)S(1)} %bitcast.77, bf16[2048,1408]{0,1:T(8,128)(2,1)} %all-gather.6.cloned.1.call-done), kind=kOutput, calls=%fused_computation.18 | convolution fusion | flops 4434001920 | bytes 14221312 | tf_op jit(solution)/shard_map/dot_general | solution.py:181
  254.8 2.1 copy.104
  256.9 41.0 %all_to_all.42 = bf16[8,768,256]{2,1,0:T(8,128)(2,1)S(1)} all-to-all(bf16[8,768,256]{2,1,0:T(8,128)(2,1)S(1)} %bitcast.67), channel_id=1, replica_groups=mesh['sp'=16,'tp'=8] {'tp'}, dimensions={0} | all-to-all | bytes 6291456 | tf_op jit(solution)/shard_map/all_to_all | solution.py:60
  298.0 0.4 convert_reduce_fusion
  298.4 0.3 copy.98
  298.7 0.4 copy-done.4
  299.2 0.9 copy.99
  (67 shorter events, 1.5 us)
Async XLA Ops:
  6.5 2.4 copy-start
  6.5 71.7 %all-gather.4.cloned.1.call-start = ((), (), s32[]{:S(2)}) async-start(), calls=%async_computation.5 | async-start | bytes 6684672 | tf_op jit(solution)/shard_map/all_gather | solution.py:29
  10.5 3.1 %copy-start.6 = (bf16[128,2048]{1,0:T(8,128)(2,1)S(1)}, bf16[128,2048]{1,0:T(8,128)(2,1)}, u32[]{:S(2)}) copy-start(bf16[128,2048]{1,0:T(8,128)(2,1)} %param.19) | copy-start | bytes 1572868
  12.3 8.1 %copy-start.8 = (bf16[128,704]{0,1:T(8,128)(2,1)S(1)}, bf16[128,704]{0,1:T(8,128)(2,1)}, u32[]{:S(2)}) copy-start(bf16[128,704]{0,1:T(8,128)(2,1)} %param.22) | copy-start | bytes 540676
  12.3 8.1 %copy-start.9 = (bf16[128,704]{0,1:T(8,128)(2,1)S(1)}, bf16[128,704]{0,1:T(8,128)(2,1)}, u32[]{:S(2)}) copy-start(bf16[128,704]{0,1:T(8,128)(2,1)} %param.21) | copy-start | bytes 540676
  14.7 132.7 %all-to-all-start.1 = ((bf16[128,8,256]{0,2,1:T(8,128)(2,1)}), bf16[128,8,256]{0,2,1:T(8,128)(2,1)}, u32[]{:S(2)}, u32[]{:S(2)}) async-start(bf16[128,8,256]{0,2,1:T(8,128)(2,1)} %bitcast.9), calls=%async_computation.1 | async-start | bytes 1048576 | tf_op jit(solution)/shard_map/all_to_all | solution.py:108
  20.5 216.2 %all-gather.6.cloned.1.call-start = ((), (), s32[]{:S(2)}) async-start(), calls=%async_computation.6 | async-start | bytes 6127616 | tf_op jit(solution)/shard_map/all_gather | solution.py:29
  87.1 4.9 %copy-start.2 = (f32[2048,768]{1,0:T(8,128)S(1)}, f32[2048,768]{1,0:T(8,128)}, u32[]{:S(2)}) copy-start(f32[2048,768]{1,0:T(8,128)} %get-tuple-element.238) | copy-start | bytes 18874372 | tf_op jit(solution)/shard_map/while
  98.1 4.7 %copy-start.2 = (f32[2048,768]{1,0:T(8,128)S(1)}, f32[2048,768]{1,0:T(8,128)}, u32[]{:S(2)}) copy-start(f32[2048,768]{1,0:T(8,128)} %get-tuple-element.238) | copy-start | bytes 18874372 | tf_op jit(solution)/shard_map/while
  108.9 4.6 %copy-start.2 = (f32[2048,768]{1,0:T(8,128)S(1)}, f32[2048,768]{1,0:T(8,128)}, u32[]{:S(2)}) copy-start(f32[2048,768]{1,0:T(8,128)} %get-tuple-element.238) | copy-start | bytes 18874372 | tf_op jit(solution)/shard_map/while
  119.6 4.6 %copy-start.2 = (f32[2048,768]{1,0:T(8,128)S(1)}, f32[2048,768]{1,0:T(8,128)}, u32[]{:S(2)}) copy-start(f32[2048,768]{1,0:T(8,128)} %get-tuple-element.238) | copy-start | bytes 18874372 | tf_op jit(solution)/shard_map/while
  130.3 4.7 %copy-start.2 = (f32[2048,768]{1,0:T(8,128)S(1)}, f32[2048,768]{1,0:T(8,128)}, u32[]{:S(2)}) copy-start(f32[2048,768]{1,0:T(8,128)} %get-tuple-element.238) | copy-start | bytes 18874372 | tf_op jit(solution)/shard_map/while
  141.0 4.6 %copy-start.2 = (f32[2048,768]{1,0:T(8,128)S(1)}, f32[2048,768]{1,0:T(8,128)}, u32[]{:S(2)}) copy-start(f32[2048,768]{1,0:T(8,128)} %get-tuple-element.238) | copy-start | bytes 18874372 | tf_op jit(solution)/shard_map/while
  147.0 7.4 %copy-start.7 = (bf16[768,256]{1,0:T(8,128)(2,1)S(1)}, bf16[768,256]{1,0:T(8,128)(2,1)}, u32[]{:S(2)}) copy-start(bf16[768,256]{1,0:T(8,128)(2,1)} %param.13) | copy-start | bytes 1179652
  148.6 25.7 %all-to-all-start = ((bf16[8,768,128]{1,2,0:T(8,128)(2,1)}), bf16[8,768,128]{1,2,0:T(8,128)(2,1)S(1)}, u32[]{:S(2)}, u32[]{:S(2)}) async-start(bf16[8,768,128]{1,2,0:T(8,128)(2,1)} %broadcast_in_dim.17), calls=%async_computation | async-start | bytes 3145728 | tf_op jit(solution)/shard_map/all_to_all | solution.py:40
  153.7 89.7 %all-gather.8.cloned.1.call-start = ((), (), s32[]{:S(2)}) async-start(), calls=%async_computation.7 | async-start | bytes 3063808 | tf_op jit(solution)/shard_map/all_gather | solution.py:183
  183.1 10.0 %copy-start.3 = (f32[768,256]{0,1:T(8,128)}, f32[768,256]{0,1:T(8,128)S(1)}, u32[]{:S(2)}) copy-start(f32[768,256]{0,1:T(8,128)S(1)} %get-tuple-element.185) | copy-start | bytes 2359300
  183.7 9.0 %all-to-all-start.2 = ((f32[8,1,768]{2,1,0:T(1,128)}), f32[8,1,768]{2,1,0:T(1,128)S(1)}, u32[]{:S(2)}, u32[]{:S(2)}) async-start(f32[8,1,768]{2,1,0:T(1,128)} %broadcast_in_dim.18), calls=%async_computation.2 | async-start | bytes 49152 | tf_op jit(solution)/shard_map/all_to_all | solution.py:40
  236.6 6.7 %copy-start.5 = (bf16[768,8,256]{0,2,1:T(8,128)(2,1)S(1)}, bf16[768,8,256]{0,2,1:T(8,128)(2,1)}, u32[]{:S(2)}) copy-start(bf16[768,8,256]{0,2,1:T(8,128)(2,1)} %copy.95) | copy-start | bytes 9437188
  256.9 43.2 %copy-start.1 = (bf16[768,256]{1,0:T(8,128)(2,1)S(1)}, bf16[768,256]{1,0:T(8,128)(2,1)}, u32[]{:S(2)}) copy-start(bf16[768,256]{1,0:T(8,128)(2,1)} %param.16) | copy-start | bytes 1179652
  298.0 1.1 copy-start.4
Sparse Core Ops, SparseCore 0:
  13.7 64.4 all-gather.3
  80.3 62.8 all-gather.5
  156.6 48.6 all-gather.7
